TPU v7x, 32 devices: a whole 2x2x4 slice. The times are simulated.
32 devices in a mesh: grp: 2 (over y), sp: 4 (over z), tp: 4 (over x, core).
Axes of the slice: x: 2, y: 2, z: 4, core: 2. Of those that a mesh axis runs over, the one named last changes fastest.
Arguments:
- hidden_in: bfloat16 [3072, 4096], P(('grp', 'sp'), 'tp'), parts along dimension 0, may hold values from -30 to 30
- in_gain: float32 [2, 4096], P(None, 'tp'), may hold values from 0.1 to 1.9
- w_value: bfloat16 [2, 4096, 2048], P(None, 'sp', 'tp'), may hold values from -0.09375 to 0.09375
- w_gate: bfloat16 [2, 4096, 2048], P(None, 'sp', 'tp'), may hold values from -0.09375 to 0.09375
- conv_taps: float32 [2, 31, 2048], P(None, None, 'tp'), may hold values from -9 to 9
- norm_gain: float32 [2, 2048], P(None, 'tp'), may hold values from 0.1 to 1.9
- norm_shift: float32 [2, 2048], P(None, 'tp'), may hold values from -3 to 3
- w_out: bfloat16 [2, 2048, 4096], P(None, 'tp', 'sp'), may hold values from -0.125 to 0.125
Outputs:
- hidden_out: bfloat16 [3072, 4096], P(('grp', 'sp'), 'tp'), parts along dimension 0
There are 2 independent parts, one for each index of `grp`. A program takes and returns all parts, laid end to end along the dimension named above; an argument that names none is the same for every part. Nothing has to cross between parts.
All inputs are finite; a program needn't handle non-finite values.
Results may differ from a plain program's by a relative error of at most 0.013.
Values may be sent and summed in bfloat16 or wider, within the bound.
A program may use at most 64 MiB of HBM per device.

v0:
```python
import jax
import jax.numpy as jnp
from jax import lax
from jax.sharding import PartitionSpec as P

D = 4096
C = 2048
epsilon = 1e-06


def passed_along(value, axis, steps):
    count = lax.axis_size(axis)
    initial, last = (max(0, -steps), min(count, count - steps))
    return lax.ppermute(value, axis, [(source, source + steps) for source in range(initial, last)])


def depthwise(extended, kernel_taps):
    conved = lax.conv_general_dilated(
        extended.astype(jnp.float32)[None],
        kernel_taps[:, None, :],
        (1,),
        [(0, 0)],
        dimension_numbers=("NWC", "WIO", "NWC"),
        feature_group_count=extended.shape[1],
        precision=lax.Precision.HIGHEST,
    )
    return conved[0]


def shards(hidden_in, in_gain, w_value, w_gate, conv_taps, norm_gain, norm_shift, w_out):
    layer_count = w_value.shape[0]
    reach_rows = conv_taps.shape[1] - 1
    value_all, gate_all = (
        lax.all_gather(w_value, "sp", axis=1, tiled=True),
        lax.all_gather(w_gate, "sp", axis=1, tiled=True),
    )
    out_all = lax.all_gather(w_out, "sp", axis=2, tiled=True)
    current = hidden_in
    for layer_idx in range(layer_count):
        widened = current.astype(jnp.float32)
        squares = lax.psum(jnp.sum(widened * widened, axis=1), "tp")
        normalized = (
            widened * lax.rsqrt(squares / D + epsilon)[:, None] * in_gain[layer_idx]
        ).astype(jnp.bfloat16)
        gathered = lax.all_gather(normalized, "tp", axis=1, tiled=True)
        value_part = jnp.dot(gathered, value_all[layer_idx], preferred_element_type=jnp.float32)
        gate_part = jnp.dot(gathered, gate_all[layer_idx], preferred_element_type=jnp.float32)
        gated = (value_part * jax.nn.sigmoid(gate_part)).astype(jnp.bfloat16)
        before = passed_along(gated[gated.shape[0] - reach_rows :], "sp", 1)
        extended = jnp.concatenate([before, gated], axis=0)
        residual = current
        conved = depthwise(extended, conv_taps[layer_idx])
        total_sum, total_squares = lax.psum(
            (jnp.sum(conved, axis=1), jnp.sum(conved * conved, axis=1)), "tp"
        )
        row_mean = total_sum / C
        spread = total_squares / C - row_mean * row_mean
        normed = (conved - row_mean[:, None]) * lax.rsqrt(spread + epsilon)[:, None] * norm_gain[
            layer_idx
        ] + norm_shift[layer_idx]
        mixed_out = jax.nn.silu(normed).astype(jnp.bfloat16)
        partial_value = jnp.dot(mixed_out, out_all[layer_idx], preferred_element_type=jnp.float32)
        summed = lax.psum_scatter(
            partial_value.astype(jnp.bfloat16), "tp", scatter_dimension=1, tiled=True
        ).astype(jnp.float32)
        current = (residual.astype(jnp.float32) + summed).astype(jnp.bfloat16)
    return current


def solution(mesh):
    placed = (
        P(("grp", "sp"), "tp"),
        P(None, "tp"),
        P(None, "sp", "tp"),
        P(None, "sp", "tp"),
        P(None, None, "tp"),
        P(None, "tp"),
        P(None, "tp"),
        P(None, "tp", "sp"),
    )
    return jax.shard_map(
        shards, mesh=mesh, in_specs=placed, out_specs=P(("grp", "sp"), "tp"), check_vma=False
    )
```

profile of v0, /device:TPU:0, one launch (start us, length us, event | category | flops | bytes accessed | tf_op | source)
XLA Modules:
  0.0 657.1 jit_solution(9422213232833642842)
XLA Ops:
  6.5 1.4 fusion.4
  7.9 8.4 %psum.42 = f32[384]{0:T(512)S(1)} all-reduce(f32[384]{0:T(512)S(1)} %fusion.4), channel_id=1, replica_groups=mesh['grp'=2,'sp'=4,'tp'=4] {'tp'}, use_global_device_ids=true, to_apply=%region_1.0 | all-reduce | flops 384 | bytes 3072 | tf_op jit(solution)/shard_map/psum | solution.py:41
  16.3 0.8 fusion.62
  17.1 2.3 fusion.6
  19.4 0.7 all-gather.10.cloned.1.call-update
  20.2 0.7 all-gather.8.cloned.1.call-update
  20.9 0.5 all-gather.12.cloned.1.call-update
  21.5 26.8 %all-gather.6.cloned.1.call-done = bf16[384,4096]{1,0:T(8,128)(2,1)} async-done(((bf16[384,1024]{1,0:T(8,128)(2,1)}), bf16[384,4096]{1,0:T(8,128)(2,1)}) %all-gather.6.cloned.1.call-update) | async-done | bytes 3145744 | tf_op jit(solution)/shard_map/all_gather | solution.py:45
  48.3 151.2 %all-gather.10.cloned.1.call-done = bf16[2,4096,512]{2,1,0:T(8,128)(2,1)} async-done(((bf16[2,1024,512]{2,1,0:T(8,128)(2,1)}), bf16[2,4096,512]{2,1,0:T(8,128)(2,1)}) %all-gather.10.cloned.1.call-update) | async-done | bytes 8388624 | tf_op jit(solution)/shard_map/all_gather | solution.py:35
  199.5 5.9 fusion.23
  205.5 143.5 %all-gather.8.cloned.1.call-done = bf16[2,4096,512]{2,1,0:T(8,128)(2,1)} async-done(((bf16[2,1024,512]{2,1,0:T(8,128)(2,1)}), bf16[2,4096,512]{2,1,0:T(8,128)(2,1)}) %all-gather.8.cloned.1.call-update) | async-done | bytes 8388624 | tf_op jit(solution)/shard_map/all_gather | solution.py:34
  349.0 4.2 fusion.25
  353.2 1.4 collective-permute-start
  354.6 1.6 collective-permute-done
  356.2 0.1 maximum_bitcast_fusion
  356.4 0.1 copy.14
  356.6 1.9 fusion.65
  358.5 0.5 copy.16
  359.0 0.1 reshape.62
  359.1 0.5 copy.15
  359.6 0.1 reshape.60
  359.7 0.2 slice_reduce_fusion.1
  359.9 6.6 all-reduce.1
  366.5 131.7 %all-gather.12.cloned.1.call-done = bf16[2,512,4096]{2,1,0:T(8,128)(2,1)} async-done(((bf16[2,512,1024]{2,1,0:T(8,128)(2,1)}), bf16[2,512,4096]{2,1,0:T(8,128)(2,1)}) %all-gather.12.cloned.1.call-update) | async-done | bytes 8388624 | tf_op jit(solution)/shard_map/all_gather | solution.py:37
  498.2 5.9 convolution_convert_fusion.1
  504.2 36.0 %reduce-scatter.3.cloned.1.call-done = bf16[384,1024]{1,0:T(8,128)(2,1)} async-done(((bf16[384,4096]{1,0:T(8,128)(2,1)}), bf16[384,1024]{1,0:T(8,128)(2,1)}) %reduce-scatter.3.cloned.1.call-update) | async-done | bytes 786448 | tf_op jit(solution)/shard_map/reduce_scatter | solution.py:63
  540.2 1.5 fusion.8
  541.6 5.8 psum.45
  547.4 2.3 fusion.10
  549.8 0.2 reduce-scatter.5.cloned.1.call-start
  550.0 29.1 %all-gather.14.cloned.1.call-done = bf16[384,4096]{1,0:T(8,128)(2,1)} async-done(((bf16[384,1024]{1,0:T(8,128)(2,1)}), bf16[384,4096]{1,0:T(8,128)(2,1)}) %all-gather.14.cloned.1.call-update) | async-done | bytes 3145744 | tf_op jit(solution)/shard_map/all_gather | solution.py:45
  579.0 5.2 fusion.21
  584.2 4.0 fusion.24
  588.3 3.4 collective-permute-start.1
  591.7 1.6 collective-permute-done.1
  593.3 0.1 maximum_bitcast_fusion.1
  593.5 0.1 copy.18
  593.7 2.0 fusion.66
  595.7 0.5 copy.20
  596.2 0.1 reshape.71
  596.3 0.1 slice_reduce_fusion
  596.5 0.5 copy.19
  597.0 0.1 reshape.69
  597.1 0.1 slice_reduce_fusion.2
  597.2 5.9 all-reduce
  603.2 5.9 convolution_convert_fusion
  609.1 38.7 %reduce-scatter.5.cloned.1.call-done = bf16[384,1024]{1,0:T(8,128)(2,1)} async-done(((bf16[384,4096]{1,0:T(8,128)(2,1)}), bf16[384,1024]{1,0:T(8,128)(2,1)}) %reduce-scatter.5.cloned.1.call-update) | async-done | bytes 786448 | tf_op jit(solution)/shard_map/reduce_scatter | solution.py:63
  647.8 2.4 fusion.11
  (40 shorter events, 0.7 us)
Async XLA Ops:
  6.5 41.8 %all-gather.6.cloned.1.call-start = ((), (), s32[]{:S(2)}) async-start(), calls=%async_computation.2 | async-start | bytes 3932160 | tf_op jit(solution)/shard_map/all_gather | solution.py:45
  19.4 2.1 copy-start.2
  19.4 180.2 %all-gather.10.cloned.1.call-start = ((), (), s32[]{:S(2)}) async-start(), calls=%async_computation.4 | async-start | bytes 10485760 | tf_op jit(solution)/shard_map/all_gather | solution.py:35
  20.1 328.8 %all-gather.8.cloned.1.call-start = ((), (), s32[]{:S(2)}) async-start(), calls=%async_computation.3 | async-start | bytes 10485760 | tf_op jit(solution)/shard_map/all_gather | solution.py:34
  20.9 477.4 %all-gather.12.cloned.1.call-start = ((), (), s32[]{:S(2)}) async-start(), calls=%async_computation.5 | async-start | bytes 10485760 | tf_op jit(solution)/shard_map/all_gather | solution.py:37
  21.4 518.8 %reduce-scatter.3.cloned.1.call-start = ((), (), s32[]{:S(2)}) async-start(), calls=%async_computation.6 | async-start | bytes 3932160 | tf_op jit(solution)/shard_map/reduce_scatter | solution.py:63
  48.3 300.6 %copy-start.4 = (bf16[384,4096]{1,0:T(8,128)(2,1)S(1)}, bf16[384,4096]{1,0:T(8,128)(2,1)}, u32[]{:S(2)}) copy-start(bf16[384,4096]{1,0:T(8,128)(2,1)} %all-gather.6.cloned.1.call-done) | copy-start | bytes 9437188
  205.5 149.1 %copy-start.3 = (f32[2,512]{1,0:T(2,128)S(1)}, f32[2,512]{1,0:T(2,128)}, u32[]{:S(2)}) copy-start(f32[2,512]{1,0:T(2,128)} %param.14) | copy-start | bytes 12292
  353.1 3.5 copy-start.6
  353.2 3.5 copy-start.7
  353.2 3.0 collective-permute-start
  504.1 36.1 %copy-start = (bf16[384,1024]{1,0:T(8,128)(2,1)S(1)}, bf16[384,1024]{1,0:T(8,128)(2,1)}, u32[]{:S(2)}) copy-start(bf16[384,1024]{1,0:T(8,128)(2,1)} %param.8) | copy-start | bytes 2359300
  504.1 74.9 %all-gather.14.cloned.1.call-start = ((), (), s32[]{:S(2)}) async-start(), calls=%async_computation.7 | async-start | bytes 3932160 | tf_op jit(solution)/shard_map/all_gather | solution.py:45
  549.8 98.0 %reduce-scatter.5.cloned.1.call-start = ((), (), s32[]{:S(2)}) async-start(), calls=%async_computation.8 | async-start | bytes 3932160 | tf_op jit(solution)/shard_map/reduce_scatter | solution.py:63
  579.0 5.2 copy-start.5
  588.3 5.0 collective-permute-start.1
  609.1 38.7 %copy-start.1 = (bf16[384,1024]{1,0:T(8,128)(2,1)S(1)}, bf16[384,1024]{1,0:T(8,128)(2,1)}, u32[]{:S(2)}) copy-start(bf16[384,1024]{1,0:T(8,128)(2,1)} %reduce-scatter.3.cloned.1.call-done) | copy-start | bytes 2359300
Sparse Core Ops, SparseCore 0:
  19.5 28.8 all-gather.5
  49.9 149.6 all-gather.9
  201.1 147.7 all-gather.7
  350.4 147.7 all-gather.11
  504.2 35.8 reduce-scatter.2
  549.9 29.1 all-gather.13
  609.2 38.5 reduce-scatter.4
where the time goes:
time: 658 us; the launch traced here: 657 us
  waiting for transfers between devices  562 us (85%)
  matrix products  35 us (5%)
  blocking collectives  26.6 us (4%)
  between operations  13.8 us (2%)
  other arithmetic  10.6 us (2%)
    all_gather x1, waiting for transfers between devices, shards(): lax.all_gather(w_gate, 'sp', axis=1, tiled=True)  151 us
    all_gather x1, waiting for transfers between devices, shards(): lax.all_gather(w_value, 'sp', axis=1, tiled=True)  143 us
    all_gather x1, waiting for transfers between devices, shards(): out_all = lax.all_gather(w_out, 'sp', axis=2, tiled=True)  132 us
    reduce_scatter x2, waiting for transfers between devices, shards(): lax.psum_scatter(partial_value.astype(jnp.bfloat16), 'tp', scatter_dimens...  74.7 us
    all_gather x2, waiting for transfers between devices, shards(): gathered = lax.all_gather(normalized, 'tp', axis=1, tiled=True)  55.9 us
    psum x2, blocking collectives, shards(): squares = lax.psum(jnp.sum(widened * widened, axis=1), 'tp')  14.1 us
  transfers between devices with their start and end apart: 9, of which 9 were waited for; matrix products, arithmetic and copies ran while one was open for 2% of the time, Pallas kernels for 0%

commit v1 on v0

--- a/solution.py
+++ b/solution.py
@@ -34,7 +34,7 @@
         lax.all_gather(w_value, "sp", axis=1, tiled=True),
         lax.all_gather(w_gate, "sp", axis=1, tiled=True),
     )
-    out_all = lax.all_gather(w_out, "sp", axis=2, tiled=True)
+    out_all = jnp.concatenate(lax.all_gather(w_out, "sp"), axis=2)
     current = hidden_in
     for layer_idx in range(layer_count):
         widened = current.astype(jnp.float32)

time: 658 us -> 684 us (1.040)
  local copies, waits for them, and re-layouts: 3.79 us -> 22.6 us
  waiting for transfers between devices: 562 us -> 569 us
    slice x0 -> x3, local copies, waits for them, and re-layouts: none -> 18.3 us  [shards(): out_all[layer_idx]]
    all_gather x1, waiting for transfers between devices: 132 us -> 143 us  [shards(): out_all = jnp.concatenate(lax.all_gather(w_out, 'sp'), axis=2)]
  transfers between devices with their start and end apart: 9 -> 9, of which waited for: 9 -> 7; matrix products, arithmetic and copies ran while one was open for 2% -> 4% of each run, Pallas kernels for 0% -> 0%
where the time goes in v1:
time: 684 us; the launch traced here: 683 us
  waiting for transfers between devices  569 us (83%)
  matrix products  34.8 us (5%)
  blocking collectives  26.9 us (4%)
  local copies, waits for them, and re-layouts  22.6 us (3%)
  between operations  13.8 us (2%)
  other arithmetic  10.6 us (2%)
    all_gather x1, waiting for transfers between devices, shards(): lax.all_gather(w_gate, 'sp', axis=1, tiled=True)  151 us
    all_gather x1, waiting for transfers between devices, shards(): lax.all_gather(w_value, 'sp', axis=1, tiled=True)  144 us
    all_gather x1, waiting for transfers between devices, shards(): out_all = jnp.concatenate(lax.all_gather(w_out, 'sp'), axis=2)  143 us
    reduce_scatter x2, waiting for transfers between devices, shards(): lax.psum_scatter(partial_value.astype(jnp.bfloat16), 'tp', scatter_dimens...  73 us
    all_gather x2, waiting for transfers between devices, shards(): gathered = lax.all_gather(normalized, 'tp', axis=1, tiled=True)  55.9 us
    slice x3, local copies, waits for them, and re-layouts, shards(): out_all[layer_idx]  18.3 us
    psum x2, blocking collectives, shards(): squares = lax.psum(jnp.sum(widened * widened, axis=1), 'tp')  14.1 us
  transfers between devices with their start and end apart: 9, of which 7 were waited for; matrix products, arithmetic and copies ran while one was open for 4% of the time, Pallas kernels for 0%

profile of v1, /device:TPU:0, one launch (start us, length us, event | category | flops | bytes accessed | tf_op | source)
XLA Modules:
  0.0 683.0 jit_solution(12178636627643781210)
XLA Ops:
  6.5 0.8 fusion.63
  7.3 1.4 fusion.4
  8.7 8.4 %psum.42 = f32[384]{0:T(512)S(1)} all-reduce(f32[384]{0:T(512)S(1)} %fusion.4), channel_id=1, replica_groups=mesh['grp'=2,'sp'=4,'tp'=4] {'tp'}, use_global_device_ids=true, to_apply=%region_1.0 | all-reduce | flops 384 | bytes 3072 | tf_op jit(solution)/shard_map/psum | solution.py:41
  17.1 2.3 fusion.6
  19.4 0.7 all-gather.11.cloned.1.call-update
  20.2 0.7 all-gather.9.cloned.1.call-update
  20.9 0.5 all-gather.15.cloned.1.call-update
  21.5 26.8 %all-gather.7.cloned.1.call-done = bf16[384,4096]{1,0:T(8,128)(2,1)} async-done(((bf16[384,1024]{1,0:T(8,128)(2,1)}), bf16[384,4096]{1,0:T(8,128)(2,1)}) %all-gather.7.cloned.1.call-update) | async-done | bytes 3145744 | tf_op jit(solution)/shard_map/all_gather | solution.py:45
  48.3 151.2 %all-gather.11.cloned.1.call-done = bf16[2,4096,512]{2,1,0:T(8,128)(2,1)} async-done(((bf16[2,1024,512]{2,1,0:T(8,128)(2,1)}), bf16[2,4096,512]{2,1,0:T(8,128)(2,1)}) %all-gather.11.cloned.1.call-update) | async-done | bytes 8388624 | tf_op jit(solution)/shard_map/all_gather | solution.py:35
  199.5 5.0 fusion.23
  204.6 144.4 %all-gather.9.cloned.1.call-done = bf16[2,4096,512]{2,1,0:T(8,128)(2,1)} async-done(((bf16[2,1024,512]{2,1,0:T(8,128)(2,1)}), bf16[2,4096,512]{2,1,0:T(8,128)(2,1)}) %all-gather.9.cloned.1.call-update) | async-done | bytes 8388624 | tf_op jit(solution)/shard_map/all_gather | solution.py:34
  349.0 4.9 fusion.25
  353.9 1.3 collective-permute-start
  355.2 143.0 %all-gather.15.cloned.1.call-done = bf16[8,512,1024]{2,1,0:T(8,128)(2,1)} async-done(((bf16[2,512,1024]{2,1,0:T(8,128)(2,1)}), bf16[8,512,1024]{2,1,0:T(8,128)(2,1)}) %all-gather.15.cloned.1.call-update) | async-done | bytes 8388624 | tf_op jit(solution)/shard_map/all_gather | solution.py:37
  498.2 5.9 fusion.62
  504.1 6.2 copy.35
  510.3 0.1 maximum_bitcast_fusion
  510.6 0.1 copy.32
  510.8 0.5 copy-done.5
  511.2 1.9 fusion.66
  513.1 0.5 copy.33
  513.6 0.1 reshape.69
  513.7 0.5 copy.34
  514.2 0.1 reshape.71
  514.3 0.2 slice_reduce_fusion.1
  514.5 6.8 %all-reduce.1 = (f32[384]{0:T(512)S(1)}, f32[384]{0:T(512)S(1)}) all-reduce(f32[384]{0:T(512)S(1)} %get-tuple-element.25, f32[384]{0:T(512)S(1)} %get-tuple-element.26), channel_id=1, replica_groups=mesh['grp'=2,'sp'=4,'tp'=4] {'tp'}, use_global_device_ids=true, to_apply=%region_5.0 | all-reduce | flops 768 | bytes 6144 | tf_op jit(solution)/shard_map/psum | solution.py:53
  521.3 5.8 convolution_convert_fusion.1
  527.3 35.1 %reduce-scatter.3.cloned.1.call-done = bf16[384,1024]{1,0:T(8,128)(2,1)} async-done(((bf16[384,4096]{1,0:T(8,128)(2,1)}), bf16[384,1024]{1,0:T(8,128)(2,1)}) %reduce-scatter.3.cloned.1.call-update) | async-done | bytes 786448 | tf_op jit(solution)/shard_map/reduce_scatter | solution.py:63
  562.4 1.5 fusion.8
  563.8 5.8 psum.45
  569.6 2.3 fusion.10
  571.9 0.2 reduce-scatter.5.cloned.1.call-start
  572.2 29.1 %all-gather.13.cloned.1.call-done = bf16[384,4096]{1,0:T(8,128)(2,1)} async-done(((bf16[384,1024]{1,0:T(8,128)(2,1)}), bf16[384,4096]{1,0:T(8,128)(2,1)}) %all-gather.13.cloned.1.call-update) | async-done | bytes 3145744 | tf_op jit(solution)/shard_map/all_gather | solution.py:45
  601.2 5.2 fusion.21
  606.4 4.0 fusion.24
  610.5 3.4 collective-permute-start.1
  613.9 6.2 copy.40
  620.1 0.1 maximum_bitcast_fusion.1
  620.3 0.1 copy.37
  620.5 2.0 fusion.67
  622.6 0.5 copy.38
  623.2 0.5 copy.39
  623.8 0.1 slice_reduce_fusion
  623.9 0.2 slice_reduce_fusion.2
  624.1 5.9 all-reduce
  630.0 5.8 convolution_convert_fusion
  635.9 37.9 %reduce-scatter.5.cloned.1.call-done = bf16[384,1024]{1,0:T(8,128)(2,1)} async-done(((bf16[384,4096]{1,0:T(8,128)(2,1)}), bf16[384,1024]{1,0:T(8,128)(2,1)}) %reduce-scatter.5.cloned.1.call-update) | async-done | bytes 786448 | tf_op jit(solution)/shard_map/reduce_scatter | solution.py:63
  673.7 2.4 fusion.11
  (41 shorter events, 0.9 us)
Async XLA Ops:
  6.5 41.8 %all-gather.7.cloned.1.call-start = ((), (), s32[]{:S(2)}) async-start(), calls=%async_computation.2 | async-start | bytes 3932160 | tf_op jit(solution)/shard_map/all_gather | solution.py:45
  19.3 2.1 copy-start.2
  19.4 2.1 copy-start.3
  19.4 180.2 %all-gather.11.cloned.1.call-start = ((), (), s32[]{:S(2)}) async-start(), calls=%async_computation.4 | async-start | bytes 10485760 | tf_op jit(solution)/shard_map/all_gather | solution.py:35
  20.1 328.8 %all-gather.9.cloned.1.call-start = ((), (), s32[]{:S(2)}) async-start(), calls=%async_computation.3 | async-start | bytes 10485760 | tf_op jit(solution)/shard_map/all_gather | solution.py:34
  20.9 477.3 %all-gather.15.cloned.1.call-start = ((), (), s32[]{:S(2)}) async-start(), calls=%async_computation.8 | async-start | bytes 10485760 | tf_op jit(solution)/shard_map/all_gather | solution.py:37
  21.4 540.9 %reduce-scatter.3.cloned.1.call-start = ((), (), s32[]{:S(2)}) async-start(), calls=%async_computation.5 | async-start | bytes 3932160 | tf_op jit(solution)/shard_map/reduce_scatter | solution.py:63
  353.9 156.4 %collective-permute-start = (bf16[30,512]{1,0:T(8,128)(2,1)S(1)}, bf16[30,512]{1,0:T(8,128)(2,1)S(1)}, u32[]{:S(2)}, u32[]{:S(2)}) collective-permute-start(bf16[30,512]{1,0:T(8,128)(2,1)S(1)} %slice.74), channel_id=1, source_target_pairs={{0,4},{4,8},{8,12},{1,5},{5,9},{9,13},{2,6},{6,10},{10,14},{3,7},{... | collective-permute-start | bytes 92168 | tf_op jit(solution)/shard_map/ppermute | solution.py:14
  510.3 0.9 copy-start.5
  510.3 0.9 copy-start.6
  527.2 35.2 %copy-start = (bf16[384,1024]{1,0:T(8,128)(2,1)S(1)}, bf16[384,1024]{1,0:T(8,128)(2,1)}, u32[]{:S(2)}) copy-start(bf16[384,1024]{1,0:T(8,128)(2,1)} %param.8) | copy-start | bytes 2359300
  527.2 74.0 %all-gather.13.cloned.1.call-start = ((), (), s32[]{:S(2)}) async-start(), calls=%async_computation.6 | async-start | bytes 3932160 | tf_op jit(solution)/shard_map/all_gather | solution.py:45
  571.9 101.8 %reduce-scatter.5.cloned.1.call-start = ((), (), s32[]{:S(2)}) async-start(), calls=%async_computation.7 | async-start | bytes 3932160 | tf_op jit(solution)/shard_map/reduce_scatter | solution.py:63
  601.2 5.2 copy-start.4
  610.5 9.6 %collective-permute-start.1 = (bf16[30,512]{1,0:T(8,128)(2,1)S(1)}, bf16[30,512]{1,0:T(8,128)(2,1)S(1)}, u32[]{:S(2)}, u32[]{:S(2)}) collective-permute-start(bf16[30,512]{1,0:T(8,128)(2,1)S(1)} %slice.81), channel_id=1, source_target_pairs={{0,4},{4,8},{8,12},{1,5},{5,9},{9,13},{2,6},{6,10},{10,14},{3,7},{... | collective-permute-start | bytes 92168 | tf_op jit(solution)/shard_map/ppermute | solution.py:14
  635.8 37.9 %copy-start.1 = (bf16[384,1024]{1,0:T(8,128)(2,1)S(1)}, bf16[384,1024]{1,0:T(8,128)(2,1)}, u32[]{:S(2)}) copy-start(bf16[384,1024]{1,0:T(8,128)(2,1)} %reduce-scatter.3.cloned.1.call-done) | copy-start | bytes 2359300
Sparse Core Ops, SparseCore 0:
  19.5 28.8 all-gather.6
  49.9 149.6 all-gather.10
  201.1 147.7 all-gather.8
  350.4 147.7 all-gather.14
  527.3 34.9 reduce-scatter.2
  572.1 29.1 all-gather.12
  636.0 37.7 reduce-scatter.4
